TPU v7x, 32 devices: a whole 2x2x4 slice. The times are simulated.
32 devices in a mesh: ep: 8 (over z, x), tp: 4 (over y, core).
Axes of the slice: x: 2, y: 2, z: 4, core: 2. Of those that a mesh axis runs over, the one named last changes fastest.
Arguments:
- mixer_query: bfloat16 [2048, 2048], P('ep', 'tp'), may hold values from -6 to 6
- mixer_forget: bfloat16 [2048, 2048], P('ep', 'tp'), may hold values from -5.5 to 5.5
- mixer_value: bfloat16 [2048, 2048], P('ep', 'tp'), may hold values from -6 to 6
- mixer_gate: bfloat16 [2048, 2048], P('ep', 'tp'), may hold values from -6 to 6
- forget_floor: float32 [2048], P('tp'), may hold values from 0.88 to 1
- head_gain: float32 [128], replicated, may hold values from 0.1 to 1.9
- mixer_proj: bfloat16 [2048, 2048], P(None, 'tp'), may hold values from -0.125 to 0.125
- expert_tokens: bfloat16 [1024, 2048], P('ep'), may hold values from -6 to 6
- expert_gain: float32 [2048], replicated, may hold values from 0.1 to 1.9
- routes: int32 [1024, 2], P('ep'), may hold values from 0 to 7, as said below
- group_logits: float32 [1024, 4], P('ep'), may hold values from -6 to 6
- choice_logits: float32 [1024, 2], P('ep'), may hold values from -6 to 6
- w_gate: bfloat16 [8, 2048, 2048], P('ep', None, 'tp'), may hold values from -0.125 to 0.125
- w_up: bfloat16 [8, 2048, 2048], P('ep', None, 'tp'), may hold values from -0.125 to 0.125
- w_down: bfloat16 [8, 2048, 2048], P('ep', None, 'tp'), may hold values from -0.125 to 0.125
Outputs:
- mixer_out: bfloat16 [2048, 2048], P('ep', 'tp')
- expert_out: bfloat16 [1024, 2048], P('ep', 'tp')
Inputs may be any that keep to these rules, and one draw needn't show every extreme that they name: `routes`: in each aligned block of 128 rows (the rows of one index of ep) no expert is named by more than 64 rows, and some expert reaches that bound in every block; the 2 experts of a row differ and lie in the same group.
All inputs are finite; a program needn't handle non-finite values.
Results may differ from a plain program's by a relative error of at most 0.01.
Values may be sent and summed in bfloat16 or wider, within the bound.
A program may use at most 64 MiB of HBM per device.

v0:
```python
import jax
import jax.numpy as jnp
from jax import lax
from jax.experimental import pallas as pl
from jax.experimental.pallas import tpu as pltpu
from jax.sharding import PartitionSpec as P

KEYDIM = 128
VDIM = 128
GROUPS = 4
TOPK = 2
PAD = 8
norm_eps = 1e-06
F32 = jnp.float32
BF16 = jnp.bfloat16
VM = pl.BlockSpec(memory_space=pltpu.VMEM)
SM = pl.BlockSpec(memory_space=pltpu.SMEM)


def tn_dot(a, b):
    return lax.dot_general(a, b, (((0,), (0,)), ((), ())), preferred_element_type=F32)


def nt_dot(a, b):
    return lax.dot_general(a, b, (((1,), (1,)), ((), ())), preferred_element_type=F32)


def silu(v):
    return v / (1.0 + jnp.exp(-v))


def local_kernel(q_ref, f_ref, v_ref, floor_ref, intra_ref, qexp_ref, pay_ref):
    length = q_ref.shape[0]
    rows = lax.broadcasted_iota(jnp.int32, (length, length), 0)
    cols = lax.broadcasted_iota(jnp.int32, (length, length), 1)
    causal = cols <= rows
    tril = causal.astype(F32)
    for h in range(q_ref.shape[1] // KEYDIM):
        at = slice(h * KEYDIM, (h + 1) * KEYDIM)
        floor = floor_ref[:, at]
        rates = (1.0 - floor) / (1.0 + jnp.exp(f_ref[:, at].astype(F32)))
        cum = jnp.dot(
            tril, jnp.log(1.0 - rates), precision=lax.Precision.HIGHEST,
            preferred_element_type=F32,
        )
        end = cum[length - 1 : length, :]
        qexp = (silu(q_ref[:, at].astype(F32)) * jnp.exp(cum)).astype(BF16)
        kexp = (rates * jnp.exp(-cum)).astype(BF16)
        kend = (rates * jnp.exp(end - cum)).astype(BF16)
        value = v_ref[:, at]
        scores = jnp.where(causal, nt_dot(qexp, kexp), 0.0).astype(BF16)
        intra_ref[:, at] = jnp.dot(scores, value, preferred_element_type=F32)
        qexp_ref[:, at] = qexp
        pay_ref[h, :VDIM, :] = tn_dot(value, kend).astype(BF16)
        pay_ref[h, VDIM:, :] = jnp.broadcast_to(jnp.exp(end), (PAD, KEYDIM)).astype(BF16)


def finish_kernel(state_ref, intra_ref, qexp_ref, gate_ref, gain_ref, out_ref):
    for h in range(intra_ref.shape[1] // VDIM):
        at = slice(h * VDIM, (h + 1) * VDIM)

        out = intra_ref[:, at] + nt_dot(qexp_ref[:, at], state_ref[h, :VDIM, :])
        scale = lax.rsqrt(jnp.mean(out * out, axis=-1, keepdims=True) + norm_eps)
        out_ref[:, at] = (
            out * scale * gain_ref[...] * silu(gate_ref[:, at].astype(F32))
        ).astype(BF16)


def dispatch_kernel(half_ref, x_ref, gain_ref, routes_ref, gl_ref, cl_ref, out_ref, wt_ref):
    rows, width = x_ref.shape
    slots = out_ref.shape[0]
    part = out_ref.shape[1]
    experts = half_ref.shape[0] - 1
    capacity = slots // experts
    group_size = experts // GROUPS
    t0 = lax.broadcasted_iota(jnp.int32, (rows, rows), 0)
    t1 = lax.broadcasted_iota(jnp.int32, (rows, rows), 1)

    def column(row):
        return jnp.sum(jnp.where(t0 == t1, row.astype(F32), 0.0), axis=-1, keepdims=True)

    route = [column(routes_ref[j : j + 1, :]).astype(jnp.int32) for j in range(TOPK)]
    ids = lax.broadcasted_iota(jnp.int32, (rows, experts), 1)
    hot = [(r == ids).astype(F32) for r in route]
    before = jnp.dot(
        (t1 < t0).astype(BF16), sum(hot).astype(BF16), preferred_element_type=F32
    )
    group_exp = [jnp.exp(column(gl_ref[g : g + 1, :])) for g in range(GROUPS)]
    group_sum = sum(group_exp)
    gids = lax.broadcasted_iota(jnp.int32, (rows, GROUPS), 1)
    member = [
        ((r >= gids * group_size) & (r < (gids + 1) * group_size)).astype(F32) for r in route
    ]
    choice = [jnp.exp(column(cl_ref[j : j + 1, :])) for j in range(TOPK)]
    slot_ids = lax.broadcasted_iota(jnp.int32, (rows, slots), 1)
    place = jnp.zeros((rows, slots), F32)
    weight = jnp.zeros((rows, slots), F32)
    for j in range(TOPK):
        rank = jnp.sum(before * hot[j], axis=-1, keepdims=True).astype(jnp.int32)
        mark = (slot_ids == route[j] * capacity + rank).astype(F32)
        within = sum(
            jnp.sum(member[j] * member[i], axis=-1, keepdims=True) * choice[i]
            for i in range(TOPK)
        )
        prob = sum(member[j][:, g : g + 1] * group_exp[g] for g in range(GROUPS)) / group_sum
        place = place + mark
        weight = weight + mark * (prob * choice[j] / within)
    high = weight.astype(BF16)
    wt_ref[0] = high
    wt_ref[1] = (weight - high.astype(F32)).astype(BF16)
    x = x_ref[...].astype(F32)
    scale = lax.rsqrt(jnp.mean(x * x, axis=-1, keepdims=True) + norm_eps)
    cols = pl.ds(pl.multiple_of(half_ref[0] * part, part), part)
    normed = (x_ref[:, cols].astype(F32) * scale * gain_ref[:, cols]).astype(BF16)
    out_ref[...] = tn_dot(place.astype(BF16), normed).astype(BF16)


def return_kernel(wt_ref, back_ref, out_ref):
    back = back_ref[...]
    out_ref[...] = (
        jnp.dot(wt_ref[0], back, preferred_element_type=F32)
        + jnp.dot(wt_ref[1], back, preferred_element_type=F32)
    ).astype(BF16)


def later_after(later, earlier):
    later = later.astype(F32)
    rows = lax.broadcasted_iota(jnp.int32, later.shape, 1)
    decay = later[:, VDIM : VDIM + 1, :]
    return (decay * earlier.astype(F32) + jnp.where(rows < VDIM, later, 0.0)).astype(BF16)


def prefix(pay, count):
    span = pay
    before = None
    step = 1
    while step < count:
        came = lax.ppermute(span, "ep", [(i, i + step) for i in range(count - step)])
        before = came if before is None else later_after(before, came)
        step *= 2
        if step < count:
            span = later_after(span, came)
    return jnp.zeros_like(pay) if before is None else before


def cost(flops, size):
    return pl.CostEstimate(flops=flops, bytes_accessed=size, transcendentals=0)


def shaped(shape, kind):
    return jax.ShapeDtypeStruct(shape, kind)


def per_device(
    mixer_query, mixer_forget, mixer_value, mixer_gate, forget_floor, head_gain, mixer_proj,
    expert_tokens, expert_gain, routes, group_logits, choice_logits, w_gate, w_up, w_down,
):
    length, width = mixer_query.shape
    heads = width // KEYDIM
    experts = lax.axis_size("ep")
    tp = lax.axis_size("tp")
    rows, model = expert_tokens.shape
    capacity = 2 * TOPK * rows // experts
    slots = experts * capacity
    split = 2
    part = model // split
    which = lax.axis_index("tp") % split
    half = jnp.full((experts + 1,), 0, jnp.int32) + which

    outgoing, wt = pl.pallas_call(
        dispatch_kernel,
        name="dispatch",
        out_shape=(shaped((slots, part), BF16), shaped((2, rows, slots), BF16)),
        in_specs=[SM, VM, VM, VM, VM, VM],
        out_specs=(VM, VM),
        cost_estimate=cost(2 * rows * slots * part, 4000000),
    )(half, expert_tokens, expert_gain[None, :], routes.T, group_logits.T, choice_logits.T)
    arrived = lax.all_to_all(
        outgoing.reshape(experts, capacity, part), "ep", split_axis=0, concat_axis=0, tiled=True
    )

    intra, qexp, pay = pl.pallas_call(
        local_kernel,
        name="local_scan",
        out_shape=(
            shaped((length, width), F32),
            shaped((length, width), BF16),
            shaped((heads, VDIM + PAD, KEYDIM), BF16),
        ),
        in_specs=[VM] * 4,
        out_specs=(VM, VM, VM),
        cost_estimate=cost(3000000000, 4000000),
    )(mixer_query, mixer_forget, mixer_value, forget_floor[None, :])
    arrived, pay = lax.optimization_barrier((arrived, pay))
    entering = prefix(pay, experts)
    mixed = pl.pallas_call(
        finish_kernel,
        name="mixer_finish",
        out_shape=shaped((length, width), BF16),
        in_specs=[VM] * 5,
        out_specs=VM,
        cost_estimate=cost(1000000000, 4000000),
    )(entering, intra, qexp, mixer_gate, head_gain[None, :])
    mixed_all = lax.all_gather(mixed, "tp", axis=1, tiled=True)

    own = arrived.reshape(slots, part)
    other = lax.ppermute(own, "tp", [(i, i ^ 1) for i in range(tp)])
    flat_in = jnp.concatenate(
        [jnp.where(which == 0, own, other), jnp.where(which == 0, other, own)], axis=1
    )
    gate_pre = jnp.dot(flat_in, w_gate[0], preferred_element_type=F32)
    up_pre = jnp.dot(flat_in, w_up[0], preferred_element_type=F32)
    hidden = (jax.nn.silu(gate_pre) * up_pre).astype(BF16)
    hidden_all = lax.all_gather(hidden, "tp", axis=1, tiled=True)
    mixer_out = jnp.dot(mixed_all, mixer_proj, preferred_element_type=F32).astype(BF16)
    down = jnp.dot(hidden_all, w_down[0], preferred_element_type=F32).astype(BF16)
    back = lax.all_to_all(
        down.reshape(experts, capacity, -1), "ep", split_axis=0, concat_axis=0, tiled=True
    ).reshape(slots, -1)
    expert_out = pl.pallas_call(
        return_kernel,
        name="weigh",
        out_shape=shaped((rows, back.shape[1]), BF16),
        in_specs=[VM, VM],
        out_specs=VM,
        cost_estimate=cost(4 * rows * slots * back.shape[1], 1000000),
    )(wt, back)
    return (mixer_out, expert_out)


def solution(mesh):
    return jax.shard_map(
        per_device,
        mesh=mesh,
        in_specs=(
            P("ep", "tp"),
            P("ep", "tp"),
            P("ep", "tp"),
            P("ep", "tp"),
            P("tp"),
            P(),
            P(None, "tp"),
            P("ep", None),
            P(),
            P("ep", None),
            P("ep", None),
            P("ep", None),
            P("ep", None, "tp"),
            P("ep", None, "tp"),
            P("ep", None, "tp"),
        ),
        out_specs=(P("ep", "tp"), P("ep", "tp")),
        check_vma=False,
    )
```

profile of v0, /device:TPU:0, one launch (start us, length us, event | category | flops | bytes accessed | tf_op | source)
XLA Modules:
  0.0 111.2 jit_solution(13398230420160067331)
XLA Ops:
  7.2 0.0 copy-start
  7.2 0.5 add.24.half_ref
  7.7 3.1 %dispatch.1 = (bf16[512,1024]{1,0:T(8,128)(2,1)}, bf16[2,128,512]{2,1,0:T(8,128)(2,1)}) custom-call(s32[9]{0:T(128)} %add.24.half_ref, bf16[128,2048]{1,0:T(8,128)(2,1)} %x_ref.1, f32[1,2048]{1,0:T(1,128)} %bitcast.35, s32[2,128]{1,0:T(2,128)} %bitcast.41, f32[4,128]{1,0:T(4,128)} %bitcast.40, f32[2,128]{1,0:T(2,128)} %bitcast.42), custom_call_target="tpu_custom_call" | custom-call | flops 134217728 | bytes 4000000 | tf_op jit(solution)/shard_map/dispatch/pallas_call | solution.py:170
  10.8 7.3 %all-to-all-start = ((bf16[8,64,1024]{2,1,0:T(8,128)(2,1)}), bf16[8,64,1024]{2,1,0:T(8,128)(2,1)S(1)}, u32[]{:S(2)}, u32[]{:S(2)}) async-start(bf16[8,64,1024]{2,1,0:T(8,128)(2,1)} %bitcast.34), calls=%async_computation | async-start | bytes 2097152 | tf_op jit(solution)/shard_map/all_to_all | solution.py:178
  18.1 0.0 all-gather.5.cloned.1.call-start
  18.2 5.1 %local_scan.1 = (f32[256,512]{1,0:T(8,128)}, bf16[256,512]{1,0:T(8,128)(2,1)}, bf16[4,136,128]{2,1,0:T(8,128)(2,1)}) custom-call(bf16[256,512]{1,0:T(8,128)(2,1)} %q_ref.1, bf16[256,512]{1,0:T(8,128)(2,1)} %f_ref.1, bf16[256,512]{1,0:T(8,128)(2,1)} %v_ref.1, f32[1,512]{1,0:T(1,128)} %bitcast.43), custom_call_target="tpu_custom_call" | custom-call | flops 3000000000 | bytes 4000000 | tf_op jit(solution)/shard_map/local_scan/pallas_call | solution.py:182
  23.3 20.6 %all-to-all-done = bf16[8,64,1024]{2,1,0:T(8,128)(2,1)S(1)} async-done(((bf16[8,64,1024]{2,1,0:T(8,128)(2,1)}), bf16[8,64,1024]{2,1,0:T(8,128)(2,1)S(1)}, u32[]{:S(2)}, u32[]{:S(2)}) %all-to-all-start) | async-done | bytes 1048608 | tf_op jit(solution)/shard_map/all_to_all | solution.py:178
  43.9 0.0 collective-permute-start.3
  43.9 2.8 %collective-permute-done.3 = bf16[512,1024]{1,0:T(8,128)(2,1)} collective-permute-done((bf16[512,1024]{1,0:T(8,128)(2,1)S(1)}, bf16[512,1024]{1,0:T(8,128)(2,1)}, u32[]{:S(2)}, u32[]{:S(2)}) %collective-permute-start.3) | collective-permute-done | bytes 1048608 | tf_op jit(solution)/shard_map/ppermute | solution.py:207
  46.7 1.4 %broadcast_select_fusion.1 = (bf16[512,1024]{1,0:T(8,128)(2,1)S(1)}, bf16[512,1024]{1,0:T(8,128)(2,1)S(1)}) fusion(bf16[512,1024]{1,0:T(8,128)(2,1)} %collective-permute-done.3, pred[]{:T(512)S(6)} %eq.6, bf16[8,64,1024]{2,1,0:T(8,128)(2,1)S(1)} %all-to-all-done), kind=kLoop, calls=%fused_computation.11 | loop fusion | flops 1048576 | bytes 4194305 | tf_op jit(solution)/shard_map/jit(_where)/select_n | solution.py:209
  48.0 0.0 copy-done
  48.1 0.0 copy-start.3
  48.1 1.2 %fusion.4 = f32[512,512]{1,0:T(8,128)S(1)} fusion(bf16[1,2048,512]{2,1,0:T(8,128)(2,1)S(1)} %copy-done, bf16[512,1024]{1,0:T(8,128)(2,1)S(1)} %get-tuple-element.17, bf16[512,1024]{1,0:T(8,128)(2,1)S(1)} %get-tuple-element.16), kind=kOutput, calls=%fused_computation.5 | convolution fusion | flops 1077936128 | bytes 5242880 | tf_op jit(solution)/shard_map/dot_general | solution.py:211
  49.3 0.3 copy-done.3
  49.6 0.0 copy-start.2
  49.6 2.1 %multiply_convert_fusion = bf16[512,512]{1,0:T(8,128)(2,1)} fusion(f32[512,512]{1,0:T(8,128)S(1)} %fusion.4, bf16[1,2048,512]{2,1,0:T(8,128)(2,1)S(1)} %copy-done.3, bf16[512,1024]{1,0:T(8,128)(2,1)S(1)} %get-tuple-element.17, bf16[512,1024]{1,0:T(8,128)(2,1)S(1)} %get-tuple-element.16), kind=kOutput, calls=%fused_computation.9 | convolution fusion | flops 1079508992 | bytes 5767168 | tf_op jit(solution)/shard_map/dot_general | solution.py:212
  51.8 0.0 all-gather.5.cloned.1.call-update
  51.8 0.0 all-gather.3.cloned.1.call-start
  51.8 0.0 copy-done.2
  51.9 3.3 %collective-permute-start = (bf16[4,136,128]{2,1,0:T(8,128)(2,1)S(1)}, bf16[4,136,128]{2,1,0:T(8,128)(2,1)S(1)}, u32[]{:S(2)}, u32[]{:S(2)}) collective-permute-start(bf16[4,136,128]{2,1,0:T(8,128)(2,1)S(1)} %copy-done.2), channel_id=1, source_target_pairs={{0,4},{4,8},{8,12},{12,16},{16,20},{20,24},{24,28},{1,5},{5,9},{9,... | collective-permute-start | bytes 417800 | tf_op jit(solution)/shard_map/ppermute | solution.py:138
  55.2 3.2 %collective-permute-done = bf16[4,136,128]{2,1,0:T(8,128)(2,1)S(1)} collective-permute-done((bf16[4,136,128]{2,1,0:T(8,128)(2,1)S(1)}, bf16[4,136,128]{2,1,0:T(8,128)(2,1)S(1)}, u32[]{:S(2)}, u32[]{:S(2)}) %collective-permute-start) | collective-permute-done | bytes 139296 | tf_op jit(solution)/shard_map/ppermute | solution.py:138
  58.4 0.1 add_convert_fusion.1
  58.5 4.1 %collective-permute-start.1 = (bf16[4,136,128]{2,1,0:T(8,128)(2,1)S(1)}, bf16[4,136,128]{2,1,0:T(8,128)(2,1)S(1)}, u32[]{:S(2)}, u32[]{:S(2)}) collective-permute-start(bf16[4,136,128]{2,1,0:T(8,128)(2,1)S(1)} %add_convert_fusion.1), channel_id=1, source_target_pairs={{0,8},{4,12},{8,16},{12,20},{16,24},{20,28},{1,9},{5,13},{9,17},{1... | collective-permute-start | bytes 417800 | tf_op jit(solution)/shard_map/ppermute | solution.py:138
  62.7 2.6 %collective-permute-done.1 = bf16[4,136,128]{2,1,0:T(8,128)(2,1)S(1)} collective-permute-done((bf16[4,136,128]{2,1,0:T(8,128)(2,1)S(1)}, bf16[4,136,128]{2,1,0:T(8,128)(2,1)S(1)}, u32[]{:S(2)}, u32[]{:S(2)}) %collective-permute-start.1) | collective-permute-done | bytes 139296 | tf_op jit(solution)/shard_map/ppermute | solution.py:138
  65.3 0.1 fusion.12
  65.4 4.1 %collective-permute-start.2 = (bf16[4,136,128]{2,1,0:T(8,128)(2,1)S(1)}, bf16[4,136,128]{2,1,0:T(8,128)(2,1)S(1)}, u32[]{:S(2)}, u32[]{:S(2)}) collective-permute-start(bf16[4,136,128]{2,1,0:T(8,128)(2,1)S(1)} %get-tuple-element.18), channel_id=1, source_target_pairs={{0,16},{4,20},{8,24},{12,28},{1,17},{5,21},{9,25},{13,29},{2,18},{... | collective-permute-start | bytes 417800 | tf_op jit(solution)/shard_map/ppermute | solution.py:138
  69.6 2.6 %collective-permute-done.2 = bf16[4,136,128]{2,1,0:T(8,128)(2,1)S(1)} collective-permute-done((bf16[4,136,128]{2,1,0:T(8,128)(2,1)S(1)}, bf16[4,136,128]{2,1,0:T(8,128)(2,1)S(1)}, u32[]{:S(2)}, u32[]{:S(2)}) %collective-permute-start.2) | collective-permute-done | bytes 139296 | tf_op jit(solution)/shard_map/ppermute | solution.py:138
  72.1 0.8 add_convert_fusion.state_ref
  72.9 2.4 %mixer_finish.1 = bf16[256,512]{1,0:T(8,128)(2,1)} custom-call(bf16[4,136,128]{2,1,0:T(8,128)(2,1)} %add_convert_fusion.state_ref, f32[256,512]{1,0:T(8,128)} %get-tuple-element.12.intra_ref, bf16[256,512]{1,0:T(8,128)(2,1)} %get-tuple-element.13.qexp_ref, bf16[256,512]{1,0:T(8,128)(2,1)} %gate_ref.1, f32[1,128]{1,0:T(1,128)} %bitcast.44), custom_call_target="tpu_custom_call" | custom-call | flops 1000000000 | bytes 4000000 | tf_op jit(solution)/shard_map/mixer_finish/pallas_call | solution.py:196
  75.3 0.0 all-gather.3.cloned.1.call-update
  75.3 0.0 all-gather.5.cloned.1.call-done
  75.3 4.3 %fusion.6 = bf16[512,512]{1,0:T(8,128)(2,1)} fusion(bf16[512,2048]{1,0:T(8,128)(2,1)} %all-gather.5.cloned.1.call-done, bf16[1,2048,512]{2,1,0:T(8,128)(2,1)} %param.29), kind=kOutput, calls=%fused_computation.7 | convolution fusion | flops 1074003968 | bytes 4718592 | tf_op jit(solution)/shard_map/dot_general | solution.py:216
  79.6 7.8 %all-to-all-start.1 = ((bf16[8,64,512]{2,1,0:T(8,128)(2,1)}), bf16[8,64,512]{2,1,0:T(8,128)(2,1)S(1)}, u32[]{:S(2)}, u32[]{:S(2)}) async-start(bf16[8,64,512]{2,1,0:T(8,128)(2,1)} %bitcast.15), calls=%async_computation.1 | async-start | bytes 1048576 | tf_op jit(solution)/shard_map/all_to_all | solution.py:217
  87.4 8.0 %all-gather.3.cloned.1.call-done = bf16[256,2048]{1,0:T(8,128)(2,1)} async-done(((bf16[256,512]{1,0:T(8,128)(2,1)}), bf16[256,2048]{1,0:T(8,128)(2,1)}) %all-gather.3.cloned.1.call-update) | async-done | bytes 1048592 | tf_op jit(solution)/shard_map/all_gather | solution.py:204
  95.4 3.3 %convolution_convert_fusion = bf16[256,512]{1,0:T(8,128)(2,1)} fusion(bf16[256,2048]{1,0:T(8,128)(2,1)} %all-gather.3.cloned.1.call-done, bf16[2048,512]{1,0:T(8,128)(2,1)} %param.21), kind=kOutput, calls=%fused_computation.8 | convolution fusion | flops 537001984 | bytes 3407872 | tf_op jit(solution)/shard_map/dot_general | solution.py:215
  98.7 2.7 %all-to-all-done.1 = bf16[8,64,512]{2,1,0:T(8,128)(2,1)S(1)} async-done(((bf16[8,64,512]{2,1,0:T(8,128)(2,1)}), bf16[8,64,512]{2,1,0:T(8,128)(2,1)S(1)}, u32[]{:S(2)}, u32[]{:S(2)}) %all-to-all-start.1) | async-done | bytes 524320 | tf_op jit(solution)/shard_map/all_to_all | solution.py:217
  101.4 0.0 copy-start.1
  101.4 0.8 copy-done.1
  102.2 2.1 %weigh.1 = bf16[128,512]{1,0:T(8,128)(2,1)} custom-call(bf16[2,128,512]{2,1,0:T(8,128)(2,1)} %get-tuple-element.14.wt_ref, bf16[512,512]{1,0:T(8,128)(2,1)} %bitcast.33), custom_call_target="tpu_custom_call" | custom-call | flops 134217728 | bytes 1000000 | tf_op jit(solution)/shard_map/weigh/pallas_call | solution.py:220
  (5 shorter events, 0.0 us)
Async XLA Ops:
  7.2 40.9 %copy-start = (bf16[1,2048,512]{2,1,0:T(8,128)(2,1)S(1)}, bf16[1,2048,512]{2,1,0:T(8,128)(2,1)}, u32[]{:S(2)}) copy-start(bf16[1,2048,512]{2,1,0:T(8,128)(2,1)} %param.27) | copy-start | bytes 6291460
  10.8 33.0 %all-to-all-start = ((bf16[8,64,1024]{2,1,0:T(8,128)(2,1)}), bf16[8,64,1024]{2,1,0:T(8,128)(2,1)S(1)}, u32[]{:S(2)}, u32[]{:S(2)}) async-start(bf16[8,64,1024]{2,1,0:T(8,128)(2,1)} %bitcast.34), calls=%async_computation | async-start | bytes 2097152 | tf_op jit(solution)/shard_map/all_to_all | solution.py:178
  18.1 57.2 %all-gather.5.cloned.1.call-start = ((), (), s32[]{:S(2)}) async-start(), calls=%async_computation.3 | async-start | bytes 2621440 | tf_op jit(solution)/shard_map/all_gather | solution.py:214
  43.9 2.8 %collective-permute-start.3 = (bf16[512,1024]{1,0:T(8,128)(2,1)S(1)}, bf16[512,1024]{1,0:T(8,128)(2,1)}, u32[]{:S(2)}, u32[]{:S(2)}) collective-permute-start(bf16[512,1024]{1,0:T(8,128)(2,1)S(1)} %bitcast.32), channel_id=1, source_target_pairs={{0,1},{1,0},{2,3},{3,2},{4,5},{5,4},{6,7},{7,6},{8,9},{9,8},{10,11... | collective-permute-start | bytes 3145736 | tf_op jit(solution)/shard_map/ppermute | solution.py:207
  48.1 1.6 %copy-start.3 = (bf16[1,2048,512]{2,1,0:T(8,128)(2,1)S(1)}, bf16[1,2048,512]{2,1,0:T(8,128)(2,1)}, u32[]{:S(2)}) copy-start(bf16[1,2048,512]{2,1,0:T(8,128)(2,1)} %param.28) | copy-start | bytes 6291460
  49.6 2.2 %copy-start.2 = (bf16[4,136,128]{2,1,0:T(8,128)(2,1)S(1)}, bf16[4,136,128]{2,1,0:T(8,128)(2,1)}, u32[]{:S(2)}) copy-start(bf16[4,136,128]{2,1,0:T(8,128)(2,1)} %get-tuple-element.11) | copy-start | bytes 417796
  51.8 43.6 %all-gather.3.cloned.1.call-start = ((), (), s32[]{:S(2)}) async-start(), calls=%async_computation.2 | async-start | bytes 1310720 | tf_op jit(solution)/shard_map/all_gather | solution.py:204
  51.9 6.6 %collective-permute-start = (bf16[4,136,128]{2,1,0:T(8,128)(2,1)S(1)}, bf16[4,136,128]{2,1,0:T(8,128)(2,1)S(1)}, u32[]{:S(2)}, u32[]{:S(2)}) collective-permute-start(bf16[4,136,128]{2,1,0:T(8,128)(2,1)S(1)} %copy-done.2), channel_id=1, source_target_pairs={{0,4},{4,8},{8,12},{12,16},{16,20},{20,24},{24,28},{1,5},{5,9},{9,... | collective-permute-start | bytes 417800 | tf_op jit(solution)/shard_map/ppermute | solution.py:138
  58.5 6.8 %collective-permute-start.1 = (bf16[4,136,128]{2,1,0:T(8,128)(2,1)S(1)}, bf16[4,136,128]{2,1,0:T(8,128)(2,1)S(1)}, u32[]{:S(2)}, u32[]{:S(2)}) collective-permute-start(bf16[4,136,128]{2,1,0:T(8,128)(2,1)S(1)} %add_convert_fusion.1), channel_id=1, source_target_pairs={{0,8},{4,12},{8,16},{12,20},{16,24},{20,28},{1,9},{5,13},{9,17},{1... | collective-permute-start | bytes 417800 | tf_op jit(solution)/shard_map/ppermute | solution.py:138
  65.4 6.7 %collective-permute-start.2 = (bf16[4,136,128]{2,1,0:T(8,128)(2,1)S(1)}, bf16[4,136,128]{2,1,0:T(8,128)(2,1)S(1)}, u32[]{:S(2)}, u32[]{:S(2)}) collective-permute-start(bf16[4,136,128]{2,1,0:T(8,128)(2,1)S(1)} %get-tuple-element.18), channel_id=1, source_target_pairs={{0,16},{4,20},{8,24},{12,28},{1,17},{5,21},{9,25},{13,29},{2,18},{... | collective-permute-start | bytes 417800 | tf_op jit(solution)/shard_map/ppermute | solution.py:138
  79.6 21.8 %all-to-all-start.1 = ((bf16[8,64,512]{2,1,0:T(8,128)(2,1)}), bf16[8,64,512]{2,1,0:T(8,128)(2,1)S(1)}, u32[]{:S(2)}, u32[]{:S(2)}) async-start(bf16[8,64,512]{2,1,0:T(8,128)(2,1)} %bitcast.15), calls=%async_computation.1 | async-start | bytes 1048576 | tf_op jit(solution)/shard_map/all_to_all | solution.py:217
  101.4 0.8 copy-start.1
Sparse Core Ops, SparseCore 0:
  51.9 21.5 all-gather.4
  75.4 19.9 all-gather.2
where the time goes:
time: 112 us; the launch traced here: 111 us
  waiting for transfers between devices  42.5 us (38%)
  starting transfers between devices  26.7 us (24%)
  between operations  14.2 us (13%)
  Pallas kernels  12.7 us (11%)
  matrix products  11 us (10%)
  other arithmetic  2.37 us (2%)
  local copies, waits for them, and re-layouts  1.68 us (2%)
    all_to_all x1, waiting for transfers between devices, per_device(): lax.all_to_all(outgoing.reshape(experts, capacity, part), 'ep', split_axi...  20.6 us
    ppermute x3, starting transfers between devices, prefix(): lax.ppermute(span, 'ep', [(i, i + step) for i in range(count - step)])  11.6 us
    ppermute x3, waiting for transfers between devices, prefix(): lax.ppermute(span, 'ep', [(i, i + step) for i in range(count - step)])  8.36 us
    all_gather x1, waiting for transfers between devices, per_device(): mixed_all = lax.all_gather(mixed, 'tp', axis=1, tiled=True)  8.01 us
    all_to_all x1, starting transfers between devices, per_device(): lax.all_to_all(down.reshape(experts, capacity, -1), 'ep', split_axis=0, c...  7.78 us
    all_to_all x1, starting transfers between devices, per_device(): lax.all_to_all(outgoing.reshape(experts, capacity, part), 'ep', split_axi...  7.28 us
    pallas_call x1, Pallas kernels, per_device(): pl.pallas_call(local_kernel, name='local_scan', out_shape=(shaped((length...  5.13 us
    dot_general x1, matrix products, per_device(): jnp.dot(hidden_all, w_down[0], preferred_element_type=F32).astype(BF16)  4.26 us
  transfers between devices with their start and end apart: 8, of which 7 were waited for; matrix products, arithmetic and copies ran while one was open for 8% of the time, Pallas kernels for 7%

commit v1 on v0

--- a/solution.py
+++ b/solution.py
@@ -9,7 +9,7 @@
 VDIM = 128
 GROUPS = 4
 TOPK = 2
-PAD = 8
+PAD = 16
 norm_eps = 1e-06
 F32 = jnp.float32
 BF16 = jnp.bfloat16
@@ -151,6 +151,473 @@
     return jax.ShapeDtypeStruct(shape, kind)
 
 
+def remote(src, dst, send, recv, device):
+    return pltpu.make_async_remote_copy(
+        src_ref=src, dst_ref=dst, send_sem=send, recv_sem=recv, device_id=device,
+        device_id_type=pl.DeviceIdType.MESH,
+    )
+
+
+def other_plane(z, k):
+    return (z % 2 + k % 2) % 2 + 2 * ((z // 2 + k // 2) % 2)
+
+
+def split3(v):
+    high = v.astype(BF16)
+    rest = v - high.astype(F32)
+    mid = rest.astype(BF16)
+    return high, mid, (rest - mid.astype(F32)).astype(BF16)
+
+
+def fused_kernel(
+    routes_ref, gl_ref, cl_ref, floor_ref, hgain_ref, egain_ref,
+    q_hbm, f_hbm, v_hbm, g_hbm, tok_hbm, wg_hbm, wu_hbm, wd_hbm, proj_hbm,
+    mixer_ref, expert_ref,
+    q_ref, f_ref, v_ref, g_ref, tok_ref, wg_ref, wu_ref, wd_ref, proj_ref,
+    disp, wsrc, wgot, flat, hid, vout, vin, ret, back, perm,
+    cum_ref, rate_ref, qexp_ref, intra_ref, pay, payin, sums, decays, first, chain_in, chain_out,
+    ent, ent_out, mix,
+    load_sem, zs, zr, ws, wr, xs, xr, cs, cr, ys, yr, hcs, hcr, vs, vr, rs, rr,
+    ps, pr, hs, hr, es, er, ms, mr,
+):
+    ep, tp = lax.axis_index("ep"), lax.axis_index("tp")
+    z, x = ep // 2, ep % 2
+    y, c = tp // 2, tp % 2
+    own = tp
+    quarter_y = (1 - y) * 2 + c
+    quarter_c = y * 2 + (1 - c)
+    quarter_d = (1 - y) * 2 + (1 - c)
+
+    def device(z_, x_, y_, c_):
+        return (z_ * 2 + x_, y_ * 2 + c_)
+
+    x_dev = device(z, 1 - x, y, c)
+    y_dev = device(z, x, 1 - y, c)
+    c_dev = device(z, x, y, 1 - c)
+    planes = [other_plane(z, k) for k in range(GROUPS)]
+    z_dev = [device(p, x, y, c) for p in planes]
+
+    loads = [
+        pltpu.make_async_copy(src, dst, load_sem.at[i])
+        for i, (src, dst) in enumerate([
+            (tok_hbm, tok_ref), (f_hbm, f_ref), (v_hbm, v_ref), (q_hbm, q_ref),
+            (wg_hbm, wg_ref), (wu_hbm, wu_ref), (g_hbm, g_ref), (wd_hbm, wd_ref),
+            (proj_hbm, proj_ref),
+        ])
+    ]
+    tok_load, f_load, v_load, q_load, wg_load, wu_load, g_load, wd_load, proj_load = loads
+    for load in loads:
+        load.start()
+    barrier = pltpu.get_barrier_semaphore()
+    for dev in z_dev[1:] + [x_dev, y_dev, c_dev]:
+        pl.semaphore_signal(
+            barrier, inc=1, device_id=dev, device_id_type=pl.DeviceIdType.MESH
+        )
+
+    rows = tok_ref.shape[0]
+    width = tok_ref.shape[1]
+    cap, part = disp.shape[1], disp.shape[2]
+    slots = GROUPS * cap
+    group_size = TOPK
+    route = [routes_ref[j : j + 1, :] for j in range(TOPK)]
+    gids = lax.broadcasted_iota(jnp.int32, (8, rows), 0)
+    member = [
+        ((r >= gids * group_size) & (r < (gids + 1) * group_size)).astype(F32) for r in route
+    ]
+    t0 = lax.broadcasted_iota(jnp.int32, (rows, rows), 0)
+    t1 = lax.broadcasted_iota(jnp.int32, (rows, rows), 1)
+    before = jnp.dot(
+        member[0].astype(BF16), (t0 < t1).astype(BF16), preferred_element_type=F32
+    )
+
+    def over_groups(v):
+        return jnp.sum(v, axis=0, keepdims=True)
+
+    rank = over_groups(before * member[0]).astype(jnp.int32)
+    group = over_groups(gids.astype(F32) * member[0]).astype(jnp.int32)
+    slot_ids = lax.broadcasted_iota(jnp.int32, (slots, rows), 0)
+    perm[...] = (slot_ids == group * cap + rank).astype(F32).astype(BF16)
+
+    group_exp = [jnp.exp(gl_ref[i : i + 1, :]) for i in range(GROUPS)]
+    group_sum = sum(group_exp)
+    choice = [jnp.exp(cl_ref[j : j + 1, :]) for j in range(TOPK)]
+    expert_weight = [0.0] * group_size
+    for j in range(TOPK):
+        within = sum(over_groups(member[j] * member[i]) * choice[i] for i in range(TOPK))
+        prob = sum(member[j][i : i + 1, :] * group_exp[i] for i in range(GROUPS)) / group_sum
+        weight = prob * choice[j] / within
+        for m in range(group_size):
+            named = route[j] == group * group_size + m
+            expert_weight[m] = expert_weight[m] + jnp.where(named, weight, 0.0)
+    sub = lax.broadcasted_iota(jnp.int32, (8, rows), 0)
+    stacked = jnp.zeros((8, rows), F32)
+    for m in range(group_size):
+        for i, piece in enumerate(split3(expert_weight[m])):
+            stacked = jnp.where(sub == 3 * m + i, piece.astype(F32), stacked)
+    stacked = stacked.astype(BF16)
+
+    tok_load.wait()
+    tokens = tok_ref[...].astype(F32)
+    scale = lax.rsqrt(jnp.mean(tokens * tokens, axis=-1, keepdims=True) + norm_eps)
+    cols = pl.ds(pl.multiple_of(c * part, part), part)
+    normed = (tok_ref[:, cols].astype(F32) * scale * egain_ref[:, cols]).astype(BF16)
+    for i in range(GROUPS):
+        chosen = perm[i * cap : (i + 1) * cap, :]
+        disp[i] = jnp.dot(chosen, normed, preferred_element_type=F32).astype(BF16)
+        got = nt_dot(stacked, chosen)
+        pair = [got[3 * m : 3 * m + 1, :] + got[3 * m + 1 : 3 * m + 2, :] + got[3 * m + 2 : 3 * m + 3, :]
+                for m in range(group_size)]
+        lanes = lax.broadcasted_iota(jnp.int32, (8, cap), 0)
+        packed = jnp.where(lanes == 0, pair[0], jnp.where(lanes == 1, pair[1], 0.0))
+        wsrc[i] = jnp.concatenate([packed, jnp.zeros((8, wsrc.shape[2] - cap), F32)], axis=1)
+    flat[0, c, x] = disp[z]
+    wgot[0] = wsrc[z]
+
+    pl.semaphore_wait(barrier, len(z_dev[1:]) + 3)
+
+    def z_send(k):
+        return remote(disp.at[planes[k]], flat.at[k, c, x], zs.at[k], zr.at[k], z_dev[k])
+
+    def w_send(k):
+        return remote(wsrc.at[planes[k]], wgot.at[k], ws.at[k], wr.at[k], z_dev[k])
+
+    def x_send(k, b):
+        return remote(flat.at[k, c, b], flat.at[k, c, b], xs.at[k], xr.at[k], x_dev)
+
+    def c_send(k, half, b, i):
+        return remote(
+            flat.at[k, half, b], flat.at[k, half, b], cs.at[k, i], cr.at[k, i], c_dev
+        )
+
+    def arrive_z(k):
+        if k > 0:
+            z_send(k).wait_recv()
+        x_send(k, x).start()
+        c_send(k, c, x, 0).start()
+
+    def arrive_x(k):
+        x_send(k, 1 - x).wait_recv()
+        c_send(k, c, 1 - x, 1).start()
+
+    def y_send(k, at):
+        return remote(hid.at[k, at], hid.at[k, at], ys.at[k], yr.at[k], y_dev)
+
+    def hc_send(k, at, i):
+        return remote(hid.at[k, at], hid.at[k, at], hcs.at[k, i], hcr.at[k, i], c_dev)
+
+    both = 2 * cap
+
+    def gate_up(k):
+        c_send(k, 1 - c, x, 0).wait_recv()
+        c_send(k, 1 - c, 1 - x, 1).wait_recv()
+        a = [flat[k, i].reshape(both, part) for i in range(2)]
+        gate = sum(
+            jnp.dot(a[i], wg_ref[i * part : (i + 1) * part, :], preferred_element_type=F32)
+            for i in range(2)
+        )
+        up = sum(
+            jnp.dot(a[i], wu_ref[i * part : (i + 1) * part, :], preferred_element_type=F32)
+            for i in range(2)
+        )
+        hid[k, own] = (silu(gate) * up).astype(BF16)
+        y_send(k, own).start()
+        hc_send(k, own, 0).start()
+
+    def arrive_y(k):
+        y_send(k, quarter_y).wait_recv()
+        hc_send(k, quarter_y, 1).start()
+
+    depth = wd_ref.shape[0] // 4
+
+    def v_send(k, b):
+        return remote(vout.at[k, b], vin.at[k], vs.at[k], vr.at[k], x_dev)
+
+    def down(k):
+        hc_send(k, quarter_c, 0).wait_recv()
+        hc_send(k, quarter_d, 1).wait_recv()
+        value = sum(
+            jnp.dot(hid[k, i], wd_ref[i * depth : (i + 1) * depth, :], preferred_element_type=F32)
+            for i in range(4)
+        ).astype(BF16)
+        vout[k, 0] = value[:cap]
+        vout[k, 1] = value[cap:]
+        v_send(k, 1 - x).start()
+
+    def r_send(k):
+        return remote(ret.at[k], back.at[z], rs.at[k], rr.at[k], z_dev[k])
+
+    def combine(k):
+        v_send(k, x).wait_recv()
+        if k > 0:
+            w_send(k).wait_recv()
+        d0 = lax.broadcasted_iota(jnp.int32, (cap, cap), 0)
+        d1 = lax.broadcasted_iota(jnp.int32, (cap, cap), 1)
+        even, odd = wgot[k, 0:1, :cap], wgot[k, 1:2, :cap]
+        mine = jnp.where(x == 0, even, odd)
+        theirs = jnp.where(x == 0, odd, even)
+
+        def column(row):
+            return jnp.sum(jnp.where(d0 == d1, row, 0.0), axis=-1, keepdims=True)
+
+        row = (
+            column(mine) * vout[k, x].astype(F32) + column(theirs) * vin[k].astype(F32)
+        ).astype(BF16)
+        if k == 0:
+            back[z] = row
+        else:
+            ret[k] = row
+            r_send(k).start()
+
+    length = q_ref.shape[0]
+    heads = q_ref.shape[1] // KEYDIM
+    lead = heads // 2
+    causal = (
+        lax.broadcasted_iota(jnp.int32, (length, length), 1)
+        <= lax.broadcasted_iota(jnp.int32, (length, length), 0)
+    )
+
+    def p_send(start):
+        return remote(pay.at[pl.ds(start, lead)], payin, ps, pr, x_dev)
+
+    def payload():
+        f_load.wait()
+        v_load.wait()
+        tril = causal.astype(F32).astype(BF16)
+        rates = (1.0 - floor_ref[...]) / (1.0 + jnp.exp(f_ref[...].astype(F32)))
+        rate_ref[...] = rates
+        cum = sum(
+            jnp.dot(tril, piece, preferred_element_type=F32)
+            for piece in split3(jnp.log(1.0 - rates))
+        )
+        cum_ref[...] = cum
+        sub = lax.broadcasted_iota(jnp.int32, (PAD, KEYDIM), 0)
+        for h in range(heads):
+            at = slice(h * KEYDIM, (h + 1) * KEYDIM)
+            end = cum[length - 1 : length, at]
+            kend = (rates[:, at] * jnp.exp(end - cum[:, at])).astype(BF16)
+            pay[h, :VDIM, :] = tn_dot(v_ref[:, at], kend).astype(BF16)
+            high, mid, _ = split3(jnp.exp(end))
+            pay[h, VDIM:, :] = jnp.where(
+                sub == 0, high.astype(F32), jnp.where(sub == 1, mid.astype(F32), 0.0)
+            ).astype(BF16)
+        p_send((1 - x) * lead).start()
+
+    def rest(h):
+        at = slice(h * KEYDIM, (h + 1) * KEYDIM)
+        cum = cum_ref[:, at]
+        qexp = (silu(q_ref[:, at].astype(F32)) * jnp.exp(cum)).astype(BF16)
+        kexp = (rate_ref[:, at] * jnp.exp(-cum)).astype(BF16)
+        scores = jnp.where(causal, nt_dot(qexp, kexp), 0.0).astype(BF16)
+        intra_ref[:, at] = jnp.dot(scores, v_ref[:, at], preferred_element_type=F32)
+        qexp_ref[:, at] = qexp
+
+    def pair_up():
+        p_send(x * lead).wait_recv()
+        for i in range(lead):
+            mine = pay[x * lead + i].astype(F32)
+            theirs = payin[i].astype(F32)
+            s0 = jnp.where(x == 0, mine, theirs)
+            s1 = jnp.where(x == 0, theirs, mine)
+            d0 = s0[VDIM : VDIM + 1, :] + s0[VDIM + 1 : VDIM + 2, :]
+            d1 = s1[VDIM : VDIM + 1, :] + s1[VDIM + 1 : VDIM + 2, :]
+            sums[i] = d1 * s0[:VDIM, :] + s1[:VDIM, :]
+            first[i] = s0[:VDIM, :]
+            decays[i, 0:8] = jnp.broadcast_to(d0, (8, KEYDIM))
+            decays[i, 8:16] = jnp.broadcast_to(d0 * d1, (8, KEYDIM))
+
+    def h_send():
+        return remote(chain_out, chain_in, hs, hr, device((z + 1) % GROUPS, x, y, c))
+
+    def e_send(start):
+        return remote(ent_out, ent.at[pl.ds(start, lead)], es, er, x_dev)
+
+    def hop(step):
+        @pl.when(z == step)
+        def _():
+            if step == 0:
+                chain_in[...] = jnp.zeros_like(chain_in)
+            else:
+                h_send().wait_recv()
+            if step < GROUPS - 1:
+                for i in range(lead):
+                    chain_out[i] = (
+                        decays[i, 8:9] * chain_in[i].astype(F32) + sums[i]
+                    ).astype(BF16)
+                h_send().start()
+            for i in range(lead):
+                came = chain_in[i].astype(F32)
+                later = decays[i, 0:1] * came + first[i]
+                ent[x * lead + i] = jnp.where(x == 0, came, later).astype(BF16)
+                ent_out[i] = jnp.where(x == 0, later, came).astype(BF16)
+            e_send(x * lead).start()
+
+    def m_send(at):
+        return remote(mix.at[at], mix.at[at], ms.at[0], mr.at[0], y_dev)
+
+    def mc_send(at, i):
+        return remote(mix.at[at], mix.at[at], ms.at[1 + i], mr.at[1 + i], c_dev)
+
+    def finish():
+        e_send((1 - x) * lead).wait_recv()
+        g_load.wait()
+        for h in range(heads):
+            at = slice(h * VDIM, (h + 1) * VDIM)
+            out = intra_ref[:, at] + nt_dot(qexp_ref[:, at], ent[h])
+            norm = lax.rsqrt(jnp.mean(out * out, axis=-1, keepdims=True) + norm_eps)
+            mix[own, :, at] = (
+                out * norm * hgain_ref[...] * silu(g_ref[:, at].astype(F32))
+            ).astype(BF16)
+        m_send(own).start()
+        mc_send(own, 0).start()
+
+    def arrive_mix():
+        m_send(quarter_y).wait_recv()
+        mc_send(quarter_y, 1).start()
+
+    def project():
+        mc_send(quarter_c, 0).wait_recv()
+        mc_send(quarter_d, 1).wait_recv()
+        proj_load.wait()
+        wide = proj_ref.shape[0] // 4
+        mixer_ref[...] = sum(
+            jnp.dot(mix[i], proj_ref[i * wide : (i + 1) * wide, :], preferred_element_type=F32)
+            for i in range(4)
+        ).astype(BF16)
+
+    for k in range(1, GROUPS):
+        z_send(k).start()
+        w_send(k).start()
+    arrive_z(0)
+    payload()
+    q_load.wait()
+    rest(0)
+    rest(1)
+    arrive_x(0)
+    arrive_z(1)
+    pair_up()
+    hop(0)
+    for h in range(2, heads):
+        rest(h)
+    wg_load.wait()
+    wu_load.wait()
+    gate_up(0)
+    arrive_z(2)
+    hop(1)
+    arrive_x(1)
+    gate_up(1)
+    arrive_y(0)
+    hop(2)
+    arrive_x(2)
+    wd_load.wait()
+    down(0)
+    arrive_z(3)
+    gate_up(2)
+    hop(3)
+    arrive_y(1)
+    combine(0)
+    down(1)
+    arrive_x(3)
+    gate_up(3)
+    arrive_y(2)
+    finish()
+    down(2)
+    combine(1)
+    combine(2)
+    arrive_y(3)
+    down(3)
+    arrive_mix()
+    combine(3)
+    project()
+    for k in range(1, GROUPS):
+        r_send(k).wait_recv()
+    expert_ref[...] = tn_dot(perm[...], back[...].reshape(slots, back.shape[2])).astype(BF16)
+
+    for k in range(GROUPS):
+        if k > 0:
+            z_send(k).wait_send()
+            w_send(k).wait_send()
+            r_send(k).wait_send()
+        x_send(k, x).wait_send()
+        c_send(k, c, x, 0).wait_send()
+        c_send(k, c, 1 - x, 1).wait_send()
+        y_send(k, own).wait_send()
+        hc_send(k, own, 0).wait_send()
+        hc_send(k, quarter_y, 1).wait_send()
+        v_send(k, 1 - x).wait_send()
+    p_send((1 - x) * lead).wait_send()
+    e_send(x * lead).wait_send()
+
+    @pl.when(z < GROUPS - 1)
+    def _():
+        h_send().wait_send()
+
+    m_send(own).wait_send()
+    mc_send(own, 0).wait_send()
+    mc_send(quarter_y, 1).wait_send()
+
+
+def fused(
+    mixer_query, mixer_forget, mixer_value, mixer_gate, forget_floor, head_gain, mixer_proj,
+    expert_tokens, expert_gain, routes, group_logits, choice_logits, w_gate, w_up, w_down,
+):
+    length, width = mixer_query.shape
+    heads = width // KEYDIM
+    lead = heads // 2
+    experts = lax.axis_size("ep")
+    rows, model = expert_tokens.shape
+    cap = 2 * TOPK * rows // experts
+    part = model // 2
+    hidden = w_gate.shape[2]
+    outs = w_down.shape[2]
+    dma, n = pltpu.SemaphoreType.DMA, GROUPS
+    any_spec = pl.BlockSpec(memory_space=pl.ANY)
+    vmem = pltpu.VMEM
+    return pl.pallas_call(
+        fused_kernel,
+        name="fused",
+        out_shape=(
+            shaped((length, mixer_proj.shape[1]), BF16),
+            shaped((rows, outs), BF16),
+        ),
+        in_specs=[VM] * 6 + [any_spec] * 9,
+        out_specs=(VM, VM),
+        scratch_shapes=[
+            vmem((length, width), BF16), vmem((length, width), BF16),
+            vmem((length, width), BF16), vmem((length, width), BF16),
+            vmem((rows, model), BF16),
+            vmem((model, hidden), BF16), vmem((model, hidden), BF16),
+            vmem(w_down.shape[1:], BF16), vmem(mixer_proj.shape, BF16),
+            vmem((n, cap, part), BF16),
+            vmem((n, 8, 128), F32), vmem((n, 8, 128), F32),
+            vmem((n, 2, 2, cap, part), BF16),
+            vmem((n, 4, 2 * cap, hidden), BF16),
+            vmem((n, 2, cap, outs), BF16), vmem((n, cap, outs), BF16),
+            vmem((n, cap, outs), BF16), vmem((n, cap, outs), BF16),
+            vmem((n * cap, rows), BF16),
+            vmem((length, width), F32), vmem((length, width), F32),
+            vmem((length, width), BF16), vmem((length, width), F32),
+            vmem((heads, VDIM + PAD, KEYDIM), BF16), vmem((lead, VDIM + PAD, KEYDIM), BF16),
+            vmem((lead, VDIM, KEYDIM), F32), vmem((lead, 16, KEYDIM), F32),
+            vmem((lead, VDIM, KEYDIM), F32),
+            vmem((lead, VDIM, KEYDIM), BF16), vmem((lead, VDIM, KEYDIM), BF16),
+            vmem((heads, VDIM, KEYDIM), BF16), vmem((lead, VDIM, KEYDIM), BF16),
+            vmem((4, length, width), BF16),
+            dma((9,)), dma((n,)), dma((n,)), dma((n,)), dma((n,)), dma((n,)), dma((n,)),
+            dma((n, 2)), dma((n, 2)), dma((n,)), dma((n,)), dma((n, 2)), dma((n, 2)),
+            dma((n,)), dma((n,)), dma((n,)), dma((n,)),
+            dma, dma, dma, dma, dma, dma, dma((3,)), dma((3,)),
+        ],
+        compiler_params=pltpu.CompilerParams(
+            collective_id=0, has_side_effects=True, vmem_limit_bytes=64000000
+        ),
+        cost_estimate=cost(8000000000, 12000000),
+    )(
+        routes.T, group_logits.T, choice_logits.T, forget_floor[None, :], head_gain[None, :],
+        expert_gain[None, :], mixer_query, mixer_forget, mixer_value, mixer_gate,
+        expert_tokens, w_gate[0], w_up[0], w_down[0], mixer_proj,
+    )
+
+
 def per_device(
     mixer_query, mixer_forget, mixer_value, mixer_gate, forget_floor, head_gain, mixer_proj,
     expert_tokens, expert_gain, routes, group_logits, choice_logits, w_gate, w_up, w_down,
@@ -229,8 +696,9 @@
 
 
 def solution(mesh):
+    paired = mesh.shape["ep"] == GROUPS * TOPK and mesh.shape["tp"] == 4
     return jax.shard_map(
-        per_device,
+        fused if paired else per_device,
         mesh=mesh,
         in_specs=(
             P("ep", "tp"),

time: 112 us -> 49.5 us (0.44)
  waiting for transfers between devices: 42.5 us -> 0 us
  Pallas kernels: 12.7 us -> 45.4 us
  starting transfers between devices: 26.7 us -> 0 us
  between operations: 14.2 us -> 0.64 us
  matrix products: 11 us -> 0 us
  other arithmetic: 2.37 us -> 0 us
  local copies, waits for them, and re-layouts: 1.68 us -> 3.24 us
    pallas_call x4 -> x1, Pallas kernels: 12.7 us -> 45.4 us  [fused(): pl.pallas_call(fused_kernel, name='fused', out_shape=(shaped((length, mix...]
    all_to_all x2 -> x0, waiting for transfers between devices: 23.3 us -> none  [the longest x1 20.6 us: per_device(): lax.all_to_all(outgoing.reshape(experts, capacity, part), 'ep', split_axi...]
    all_to_all x2 -> x0, starting transfers between devices: 15.1 us -> none  [the longest x1 7.78 us: per_device(): lax.all_to_all(down.reshape(experts, capacity, -1), 'ep', split_axis=0, c...]
    ppermute x4 -> x0, starting transfers between devices: 11.6 us -> none  [the longest x3 11.6 us: prefix(): lax.ppermute(span, 'ep', [(i, i + step) for i in range(count - step)])]
    ppermute x4 -> x0, waiting for transfers between devices: 11.2 us -> none  [the longest x3 8.36 us: prefix(): lax.ppermute(span, 'ep', [(i, i + step) for i in range(count - step)])]
    dot_general x4 -> x0, matrix products: 11 us -> none  [the longest x1 4.26 us: per_device(): jnp.dot(hidden_all, w_down[0], preferred_element_type=F32).astype(BF16)]
    all_gather x2 -> x0, waiting for transfers between devices: 8.03 us -> none  [the longest x1 8.01 us: per_device(): mixed_all = lax.all_gather(mixed, 'tp', axis=1, tiled=True)]
    unnamed x8 -> x2, local copies, waits for them, and re-layouts: 1.15 us -> 3.24 us
  transfers between devices with their start and end apart: 8 -> 0, of which waited for: 7 -> 0; matrix products, arithmetic and copies ran while one was open for 8% -> 0% of each run, Pallas kernels for 7% -> 0%
where the time goes in v1:
time: 49.5 us; the launch traced here: 49.3 us
  Pallas kernels  45.4 us (92%)
  local copies, waits for them, and re-layouts  3.24 us (7%)
  between operations  0.64 us (1%)
    pallas_call x1, Pallas kernels, fused(): pl.pallas_call(fused_kernel, name='fused', out_shape=(shaped((length, mix...  45.4 us
    unnamed x2, local copies, waits for them, and re-layouts  3.24 us

profile of v1, /device:TPU:0, one launch (start us, length us, event | category | flops | bytes accessed | tf_op | source)
XLA Modules:
  0.0 49.3 jit_solution(18429795017162330464)
XLA Ops:
  0.6 45.4 %fused.1 = (bf16[256,512]{1,0:T(8,128)(2,1)}, bf16[128,512]{1,0:T(8,128)(2,1)}) custom-call(s32[2,128]{1,0:T(2,128)} %bitcast.15, f32[4,128]{1,0:T(4,128)} %bitcast.13, f32[2,128]{1,0:T(2,128)} %bitcast.16, f32[1,512]{1,0:T(1,128)} %bitcast.14, f32[1,128]{1,0:T(1,128)} %bitcast.17, f32[1,2048]{1,0:T(1,128)} %bitcast.12, bf16[256,512]{1,0:T(8,128)(2,1)} %q_hbm.1, ...), custom_call_target="tpu_custom_call" | custom-call | flops 8000000000 | bytes 12000000 | tf_op jit(solution)/shard_map/fused/pallas_call | solution.py:575
  46.1 1.7 %copy.19 = bf16[256,512]{1,0:T(8,128)(2,1)} copy(bf16[256,512]{1,0:T(8,128)(2,1)} %get-tuple-element.4) | data formatting | bytes 524288
  47.8 1.6 %copy.20 = bf16[128,512]{1,0:T(8,128)(2,1)} copy(bf16[128,512]{1,0:T(8,128)(2,1)} %get-tuple-element.5) | data formatting | bytes 262144

commit v2 on v1

--- a/solution.py
+++ b/solution.py
@@ -9,6 +9,7 @@
 VDIM = 128
 GROUPS = 4
 TOPK = 2
+SPLIT = 2
 PAD = 16
 norm_eps = 1e-06
 F32 = jnp.float32
@@ -170,15 +171,16 @@
 
 
 def fused_kernel(
-    routes_ref, gl_ref, cl_ref, floor_ref, hgain_ref, egain_ref,
+    routes_hbm, gl_hbm, cl_hbm, floor_hbm, hgain_hbm, egain_hbm,
     q_hbm, f_hbm, v_hbm, g_hbm, tok_hbm, wg_hbm, wu_hbm, wd_hbm, proj_hbm,
     mixer_ref, expert_ref,
+    routes_ref, gl_ref, cl_ref, floor_ref, hgain_ref, egain_ref,
     q_ref, f_ref, v_ref, g_ref, tok_ref, wg_ref, wu_ref, wd_ref, proj_ref,
     disp, wsrc, wgot, flat, hid, vout, vin, ret, back, perm,
     cum_ref, rate_ref, qexp_ref, intra_ref, pay, payin, sums, decays, first, chain_in, chain_out,
     ent, ent_out, mix,
     load_sem, zs, zr, ws, wr, xs, xr, cs, cr, ys, yr, hcs, hcr, vs, vr, rs, rr,
-    ps, pr, hs, hr, es, er, ms, mr,
+    ps, pr, hs, hr, es, er, ms, mr, mcs, mcr, ds, dr,
 ):
     ep, tp = lax.axis_index("ep"), lax.axis_index("tp")
     z, x = ep // 2, ep % 2
@@ -200,12 +202,16 @@
     loads = [
         pltpu.make_async_copy(src, dst, load_sem.at[i])
         for i, (src, dst) in enumerate([
-            (tok_hbm, tok_ref), (f_hbm, f_ref), (v_hbm, v_ref), (q_hbm, q_ref),
+            (routes_hbm, routes_ref), (gl_hbm, gl_ref), (cl_hbm, cl_ref),
+            (tok_hbm, tok_ref), (egain_hbm, egain_ref), (floor_hbm, floor_ref), (f_hbm, f_ref), (v_hbm, v_ref), (q_hbm, q_ref),
             (wg_hbm, wg_ref), (wu_hbm, wu_ref), (g_hbm, g_ref), (wd_hbm, wd_ref),
-            (proj_hbm, proj_ref),
+            (proj_hbm, proj_ref), (hgain_hbm, hgain_ref),
         ])
     ]
-    tok_load, f_load, v_load, q_load, wg_load, wu_load, g_load, wd_load, proj_load = loads
+    (
+        routes_load, gl_load, cl_load, tok_load, egain_load, floor_load, f_load, v_load, q_load,
+        wg_load, wu_load, g_load, wd_load, proj_load, hgain_load,
+    ) = loads
     for load in loads:
         load.start()
     barrier = pltpu.get_barrier_semaphore()
@@ -219,6 +225,9 @@
     cap, part = disp.shape[1], disp.shape[2]
     slots = GROUPS * cap
     group_size = TOPK
+    routes_load.wait()
+    gl_load.wait()
+    cl_load.wait()
     route = [routes_ref[j : j + 1, :] for j in range(TOPK)]
     gids = lax.broadcasted_iota(jnp.int32, (8, rows), 0)
     member = [
@@ -257,6 +266,7 @@
     stacked = stacked.astype(BF16)
 
     tok_load.wait()
+    egain_load.wait()
     tokens = tok_ref[...].astype(F32)
     scale = lax.rsqrt(jnp.mean(tokens * tokens, axis=-1, keepdims=True) + norm_eps)
     cols = pl.ds(pl.multiple_of(c * part, part), part)
@@ -275,79 +285,108 @@
 
     pl.semaphore_wait(barrier, len(z_dev[1:]) + 3)
 
+    half_part = part // 2
+    my_cols = pl.ds(pl.multiple_of(y * half_part, half_part), half_part)
+    other_cols = pl.ds(pl.multiple_of((1 - y) * half_part, half_part), half_part)
+    block = [x, 1 - x]
+
+    def piece(k, b, at=my_cols):
+        return flat.at[k, c, b, :, at] if k == SPLIT else flat.at[k, c, b]
+
     def z_send(k):
-        return remote(disp.at[planes[k]], flat.at[k, c, x], zs.at[k], zr.at[k], z_dev[k])
+        rows_of = disp.at[planes[k], :, my_cols] if k == SPLIT else disp.at[planes[k]]
+        return remote(rows_of, piece(k, x), zs.at[k], zr.at[k], z_dev[k])
 
     def w_send(k):
         return remote(wsrc.at[planes[k]], wgot.at[k], ws.at[k], wr.at[k], z_dev[k])
 
     def x_send(k, b):
-        return remote(flat.at[k, c, b], flat.at[k, c, b], xs.at[k], xr.at[k], x_dev)
-
-    def c_send(k, half, b, i):
-        return remote(
-            flat.at[k, half, b], flat.at[k, half, b], cs.at[k, i], cr.at[k, i], c_dev
-        )
+        return remote(piece(k, b), piece(k, b), xs.at[k], xr.at[k], x_dev)
+
+    def d_send(i, at):
+        ref = piece(SPLIT, block[i], at)
+        return remote(ref, ref, ds.at[i], dr.at[i], y_dev)
+
+    def c_send(k, i, half):
+        ref = flat.at[k, half, block[i]]
+        return remote(ref, ref, cs.at[k, i], cr.at[k, i], c_dev)
 
     def arrive_z(k):
-        if k > 0:
-            z_send(k).wait_recv()
+        z_send(k).wait_recv()
         x_send(k, x).start()
-        c_send(k, c, x, 0).start()
+        if k == SPLIT:
+            d_send(0, my_cols).start()
+        else:
+            c_send(k, 0, c).start()
 
     def arrive_x(k):
         x_send(k, 1 - x).wait_recv()
-        c_send(k, c, 1 - x, 1).start()
-
-    def y_send(k, at):
-        return remote(hid.at[k, at], hid.at[k, at], ys.at[k], yr.at[k], y_dev)
-
-    def hc_send(k, at, i):
-        return remote(hid.at[k, at], hid.at[k, at], hcs.at[k, i], hcr.at[k, i], c_dev)
-
-    both = 2 * cap
-
-    def gate_up(k):
-        c_send(k, 1 - c, x, 0).wait_recv()
-        c_send(k, 1 - c, 1 - x, 1).wait_recv()
-        a = [flat[k, i].reshape(both, part) for i in range(2)]
+        if k == SPLIT:
+            d_send(1, my_cols).start()
+        else:
+            c_send(k, 1, c).start()
+
+    def arrive_d(i):
+        d_send(i, other_cols).wait_recv()
+        c_send(SPLIT, i, c).start()
+
+    def y_send(k, i, at):
+        ref = hid.at[k, block[i], at]
+        return remote(ref, ref, ys.at[k, i], yr.at[k, i], y_dev)
+
+    def hc_send(k, i, at, n):
+        ref = hid.at[k, block[i], at]
+        return remote(ref, ref, hcs.at[k, i, n], hcr.at[k, i, n], c_dev)
+
+    def gate_up(*blocks):
+        for k, i in blocks:
+            c_send(k, i, 1 - c).wait_recv()
+        a = [
+            jnp.concatenate([flat[k, n, block[i]] for k, i in blocks], axis=0) for n in range(2)
+        ]
         gate = sum(
-            jnp.dot(a[i], wg_ref[i * part : (i + 1) * part, :], preferred_element_type=F32)
-            for i in range(2)
+            jnp.dot(a[n], wg_ref[n * part : (n + 1) * part, :], preferred_element_type=F32)
+            for n in range(2)
         )
         up = sum(
-            jnp.dot(a[i], wu_ref[i * part : (i + 1) * part, :], preferred_element_type=F32)
-            for i in range(2)
+            jnp.dot(a[n], wu_ref[n * part : (n + 1) * part, :], preferred_element_type=F32)
+            for n in range(2)
         )
-        hid[k, own] = (silu(gate) * up).astype(BF16)
-        y_send(k, own).start()
-        hc_send(k, own, 0).start()
-
-    def arrive_y(k):
-        y_send(k, quarter_y).wait_recv()
-        hc_send(k, quarter_y, 1).start()
+        act = (silu(gate) * up).astype(BF16)
+        for m, (k, i) in enumerate(blocks):
+            hid[k, block[i], own] = act[m * cap : (m + 1) * cap]
+            y_send(k, i, own).start()
+            hc_send(k, i, own, 0).start()
+
+    def arrive_y(k, i):
+        y_send(k, i, quarter_y).wait_recv()
+        hc_send(k, i, quarter_y, 1).start()
 
     depth = wd_ref.shape[0] // 4
 
-    def v_send(k, b):
-        return remote(vout.at[k, b], vin.at[k], vs.at[k], vr.at[k], x_dev)
+    def v_send(k):
+        return remote(vout.at[k, 1], vin.at[k], vs.at[k], vr.at[k], x_dev)
 
     def down(k):
-        hc_send(k, quarter_c, 0).wait_recv()
-        hc_send(k, quarter_d, 1).wait_recv()
+        for i in range(2):
+            hc_send(k, i, quarter_c, 0).wait_recv()
+            hc_send(k, i, quarter_d, 1).wait_recv()
         value = sum(
-            jnp.dot(hid[k, i], wd_ref[i * depth : (i + 1) * depth, :], preferred_element_type=F32)
-            for i in range(4)
+            jnp.dot(
+                jnp.concatenate([hid[k, block[i], n] for i in range(2)], axis=0),
+                wd_ref[n * depth : (n + 1) * depth, :], preferred_element_type=F32,
+            )
+            for n in range(4)
         ).astype(BF16)
         vout[k, 0] = value[:cap]
         vout[k, 1] = value[cap:]
-        v_send(k, 1 - x).start()
+        v_send(k).start()
 
     def r_send(k):
         return remote(ret.at[k], back.at[z], rs.at[k], rr.at[k], z_dev[k])
 
     def combine(k):
-        v_send(k, x).wait_recv()
+        v_send(k).wait_recv()
         if k > 0:
             w_send(k).wait_recv()
         d0 = lax.broadcasted_iota(jnp.int32, (cap, cap), 0)
@@ -360,7 +399,7 @@
             return jnp.sum(jnp.where(d0 == d1, row, 0.0), axis=-1, keepdims=True)
 
         row = (
-            column(mine) * vout[k, x].astype(F32) + column(theirs) * vin[k].astype(F32)
+            column(mine) * vout[k, 0].astype(F32) + column(theirs) * vin[k].astype(F32)
         ).astype(BF16)
         if k == 0:
             back[z] = row
@@ -380,6 +419,7 @@
         return remote(pay.at[pl.ds(start, lead)], payin, ps, pr, x_dev)
 
     def payload():
+        floor_load.wait()
         f_load.wait()
         v_load.wait()
         tril = causal.astype(F32).astype(BF16)
@@ -451,83 +491,107 @@
                 ent_out[i] = jnp.where(x == 0, later, came).astype(BF16)
             e_send(x * lead).start()
 
-    def m_send(at):
-        return remote(mix.at[at], mix.at[at], ms.at[0], mr.at[0], y_dev)
-
-    def mc_send(at, i):
-        return remote(mix.at[at], mix.at[at], ms.at[1 + i], mr.at[1 + i], c_dev)
-
-    def finish():
+    mix_rows = length // 2
+
+    def m_send(j, at):
+        ref = mix.at[at, pl.ds(j * mix_rows, mix_rows)]
+        return remote(ref, ref, ms.at[j], mr.at[j], y_dev)
+
+    def mc_send(j, at, n):
+        ref = mix.at[at, pl.ds(j * mix_rows, mix_rows)]
+        return remote(ref, ref, mcs.at[j, n], mcr.at[j, n], c_dev)
+
+    def arrive_ent():
         e_send((1 - x) * lead).wait_recv()
-        g_load.wait()
+
+    def finish(j):
+        to = slice(j * mix_rows, (j + 1) * mix_rows)
         for h in range(heads):
             at = slice(h * VDIM, (h + 1) * VDIM)
-            out = intra_ref[:, at] + nt_dot(qexp_ref[:, at], ent[h])
+            out = intra_ref[to, at] + nt_dot(qexp_ref[to, at], ent[h])
             norm = lax.rsqrt(jnp.mean(out * out, axis=-1, keepdims=True) + norm_eps)
-            mix[own, :, at] = (
-                out * norm * hgain_ref[...] * silu(g_ref[:, at].astype(F32))
+            mix[own, to, at] = (
+                out * norm * hgain_ref[...] * silu(g_ref[to, at].astype(F32))
             ).astype(BF16)
-        m_send(own).start()
-        mc_send(own, 0).start()
-
-    def arrive_mix():
-        m_send(quarter_y).wait_recv()
-        mc_send(quarter_y, 1).start()
-
-    def project():
-        mc_send(quarter_c, 0).wait_recv()
-        mc_send(quarter_d, 1).wait_recv()
-        proj_load.wait()
+        m_send(j, own).start()
+        mc_send(j, own, 0).start()
+
+    def arrive_mix(j):
+        m_send(j, quarter_y).wait_recv()
+        mc_send(j, quarter_y, 1).start()
+
+    def project(j):
+        mc_send(j, quarter_c, 0).wait_recv()
+        mc_send(j, quarter_d, 1).wait_recv()
+        to = slice(j * mix_rows, (j + 1) * mix_rows)
         wide = proj_ref.shape[0] // 4
-        mixer_ref[...] = sum(
-            jnp.dot(mix[i], proj_ref[i * wide : (i + 1) * wide, :], preferred_element_type=F32)
+        mixer_ref[to, :] = sum(
+            jnp.dot(mix[i, to, :], proj_ref[i * wide : (i + 1) * wide, :], preferred_element_type=F32)
             for i in range(4)
         ).astype(BF16)
 
+    for k in (2, 1, 3):
+        z_send(k).start()
+    x_send(0, x).start()
+    c_send(0, 0, c).start()
     for k in range(1, GROUPS):
-        z_send(k).start()
         w_send(k).start()
-    arrive_z(0)
     payload()
     q_load.wait()
     rest(0)
     rest(1)
+    wg_load.wait()
+    wu_load.wait()
+    gate_up((0, 0))
+    for h in range(2, heads):
+        rest(h)
+    arrive_z(2)
     arrive_x(0)
-    arrive_z(1)
     pair_up()
     hop(0)
-    for h in range(2, heads):
-        rest(h)
-    wg_load.wait()
-    wu_load.wait()
-    gate_up(0)
-    arrive_z(2)
+    arrive_y(0, 0)
+    arrive_z(1)
+    gate_up((0, 1))
+    arrive_d(0)
+    gate_up((1, 0))
+    arrive_x(2)
     hop(1)
+    gate_up((2, 0))
+    arrive_y(0, 1)
     arrive_x(1)
-    gate_up(1)
-    arrive_y(0)
-    hop(2)
-    arrive_x(2)
+    arrive_z(3)
+    arrive_y(1, 0)
+    arrive_d(1)
+    gate_up((1, 1), (3, 0))
     wd_load.wait()
     down(0)
-    arrive_z(3)
-    gate_up(2)
+    hop(2)
+    gate_up((2, 1))
+    arrive_y(2, 0)
+    arrive_x(3)
+    arrive_y(1, 1)
     hop(3)
-    arrive_y(1)
+    arrive_y(3, 0)
+    gate_up((3, 1))
     combine(0)
+    arrive_y(2, 1)
     down(1)
-    arrive_x(3)
-    gate_up(3)
-    arrive_y(2)
-    finish()
+    arrive_ent()
+    g_load.wait()
+    hgain_load.wait()
+    finish(0)
+    finish(1)
     down(2)
     combine(1)
+    arrive_y(3, 1)
     combine(2)
-    arrive_y(3)
     down(3)
-    arrive_mix()
+    arrive_mix(0)
+    proj_load.wait()
     combine(3)
-    project()
+    project(0)
+    arrive_mix(1)
+    project(1)
     for k in range(1, GROUPS):
         r_send(k).wait_recv()
     expert_ref[...] = tn_dot(perm[...], back[...].reshape(slots, back.shape[2])).astype(BF16)
@@ -538,12 +602,17 @@
             w_send(k).wait_send()
             r_send(k).wait_send()
         x_send(k, x).wait_send()
-        c_send(k, c, x, 0).wait_send()
-        c_send(k, c, 1 - x, 1).wait_send()
-        y_send(k, own).wait_send()
-        hc_send(k, own, 0).wait_send()
-        hc_send(k, quarter_y, 1).wait_send()
-        v_send(k, 1 - x).wait_send()
+        v_send(k).wait_send()
+        for i in range(2):
+            c_send(k, i, c).wait_send()
+            y_send(k, i, own).wait_send()
+            hc_send(k, i, own, 0).wait_send()
+            hc_send(k, i, quarter_y, 1).wait_send()
+    for i in range(2):
+        d_send(i, my_cols).wait_send()
+        m_send(i, own).wait_send()
+        mc_send(i, own, 0).wait_send()
+        mc_send(i, quarter_y, 1).wait_send()
     p_send((1 - x) * lead).wait_send()
     e_send(x * lead).wait_send()
 
@@ -551,9 +620,16 @@
     def _():
         h_send().wait_send()
 
-    m_send(own).wait_send()
-    mc_send(own, 0).wait_send()
-    mc_send(quarter_y, 1).wait_send()
+
+def emit_kernel(mixer_ref, expert_ref, mixer_out, expert_out, sem):
+    copies = [
+        pltpu.make_async_copy(mixer_ref, mixer_out, sem.at[0]),
+        pltpu.make_async_copy(expert_ref, expert_out, sem.at[1]),
+    ]
+    for copy in copies:
+        copy.start()
+    for copy in copies:
+        copy.wait()
 
 
 def fused(
@@ -572,16 +648,18 @@
     dma, n = pltpu.SemaphoreType.DMA, GROUPS
     any_spec = pl.BlockSpec(memory_space=pl.ANY)
     vmem = pltpu.VMEM
-    return pl.pallas_call(
+    mixer_out, expert_out = pl.pallas_call(
         fused_kernel,
         name="fused",
         out_shape=(
-            shaped((length, mixer_proj.shape[1]), BF16),
-            shaped((rows, outs), BF16),
+            vmem((length, mixer_proj.shape[1]), BF16),
+            vmem((rows, outs), BF16),
         ),
-        in_specs=[VM] * 6 + [any_spec] * 9,
+        in_specs=[any_spec] * 15,
         out_specs=(VM, VM),
         scratch_shapes=[
+            vmem((TOPK, rows), jnp.int32), vmem((GROUPS, rows), F32), vmem((TOPK, rows), F32),
+            vmem((1, width), F32), vmem((1, VDIM), F32), vmem((1, model), F32),
             vmem((length, width), BF16), vmem((length, width), BF16),
             vmem((length, width), BF16), vmem((length, width), BF16),
             vmem((rows, model), BF16),
@@ -590,7 +668,7 @@
             vmem((n, cap, part), BF16),
             vmem((n, 8, 128), F32), vmem((n, 8, 128), F32),
             vmem((n, 2, 2, cap, part), BF16),
-            vmem((n, 4, 2 * cap, hidden), BF16),
+            vmem((n, 2, 4, cap, hidden), BF16),
             vmem((n, 2, cap, outs), BF16), vmem((n, cap, outs), BF16),
             vmem((n, cap, outs), BF16), vmem((n, cap, outs), BF16),
             vmem((n * cap, rows), BF16),
@@ -602,10 +680,11 @@
             vmem((lead, VDIM, KEYDIM), BF16), vmem((lead, VDIM, KEYDIM), BF16),
             vmem((heads, VDIM, KEYDIM), BF16), vmem((lead, VDIM, KEYDIM), BF16),
             vmem((4, length, width), BF16),
-            dma((9,)), dma((n,)), dma((n,)), dma((n,)), dma((n,)), dma((n,)), dma((n,)),
-            dma((n, 2)), dma((n, 2)), dma((n,)), dma((n,)), dma((n, 2)), dma((n, 2)),
+            dma((15,)), dma((n,)), dma((n,)), dma((n,)), dma((n,)), dma((n,)), dma((n,)),
+            dma((n, 2)), dma((n, 2)), dma((n, 2)), dma((n, 2)), dma((n, 2, 2)), dma((n, 2, 2)),
             dma((n,)), dma((n,)), dma((n,)), dma((n,)),
-            dma, dma, dma, dma, dma, dma, dma((3,)), dma((3,)),
+            dma, dma, dma, dma, dma, dma, dma((2,)), dma((2,)), dma((2, 2)), dma((2, 2)),
+            dma((2,)), dma((2,)),
         ],
         compiler_params=pltpu.CompilerParams(
             collective_id=0, has_side_effects=True, vmem_limit_bytes=64000000
@@ -616,6 +695,16 @@
         expert_gain[None, :], mixer_query, mixer_forget, mixer_value, mixer_gate,
         expert_tokens, w_gate[0], w_up[0], w_down[0], mixer_proj,
     )
+    return pl.pallas_call(
+        emit_kernel,
+        name="emit",
+        out_shape=(shaped(mixer_out.shape, BF16), shaped(expert_out.shape, BF16)),
+        in_specs=[any_spec, any_spec],
+        out_specs=(any_spec, any_spec),
+        scratch_shapes=[dma((2,))],
+        compiler_params=pltpu.CompilerParams(vmem_limit_bytes=1000000),
+        cost_estimate=cost(1000000, 800000),
+    )(mixer_out, expert_out)
 
 
 def per_device(

time: 49.5 us -> 43 us (0.87)
  local copies, waits for them, and re-layouts: 3.24 us -> 0 us
  Pallas kernels: 45.4 us -> 42.2 us
    unnamed x2 -> x0, local copies, waits for them, and re-layouts: 3.24 us -> none
    pallas_call x1 -> x2, Pallas kernels: 45.4 us -> 42.2 us  [the longest x1 41.5 us: fused(): pl.pallas_call(fused_kernel, name='fused', out_shape=(vmem((length, mixer...]
where the time goes in v2:
time: 43 us; the launch traced here: 42.9 us
  Pallas kernels  42.2 us (98%)
  between operations  0.64 us (1%)
    pallas_call x1, Pallas kernels, fused(): pl.pallas_call(fused_kernel, name='fused', out_shape=(vmem((length, mixer...  41.5 us

profile of v2, /device:TPU:0, one launch (start us, length us, event | category | flops | bytes accessed | tf_op | source)
XLA Modules:
  0.0 42.9 jit_solution(12846779581399773755)
XLA Ops:
  0.6 41.5 %fused.1 = (bf16[256,512]{1,0:T(8,128)(2,1)S(1)}, bf16[128,512]{1,0:T(8,128)(2,1)S(1)}) custom-call(s32[2,128]{1,0:T(2,128)} %bitcast.15, f32[4,128]{1,0:T(4,128)} %bitcast.13, f32[2,128]{1,0:T(2,128)} %bitcast.16, f32[1,512]{1,0:T(1,128)} %bitcast.14, f32[1,128]{1,0:T(1,128)} %bitcast.17, f32[1,2048]{1,0:T(1,128)} %bitcast.12, bf16[256,512]{1,0:T(8,128)(2,1)} %q_hbm.1, ...), custom_call_target="tpu_custom_call" | custom-call | flops 8000000000 | bytes 12000000 | tf_op jit(solution)/shard_map/fused/pallas_call | solution.py:651
  42.1 0.8 %emit.1 = (bf16[256,512]{1,0:T(8,128)(2,1)}, bf16[128,512]{1,0:T(8,128)(2,1)}) custom-call(bf16[256,512]{1,0:T(8,128)(2,1)S(1)} %get-tuple-element.4.mixer_ref, bf16[128,512]{1,0:T(8,128)(2,1)S(1)} %get-tuple-element.5.expert_ref), custom_call_target="tpu_custom_call" | custom-call | flops 1000000 | bytes 800000 | tf_op jit(solution)/shard_map/emit/pallas_call | solution.py:698

commit v3 on v2

--- a/solution.py
+++ b/solution.py
@@ -226,8 +226,6 @@
     slots = GROUPS * cap
     group_size = TOPK
     routes_load.wait()
-    gl_load.wait()
-    cl_load.wait()
     route = [routes_ref[j : j + 1, :] for j in range(TOPK)]
     gids = lax.broadcasted_iota(jnp.int32, (8, rows), 0)
     member = [
@@ -247,24 +245,6 @@
     slot_ids = lax.broadcasted_iota(jnp.int32, (slots, rows), 0)
     perm[...] = (slot_ids == group * cap + rank).astype(F32).astype(BF16)
 
-    group_exp = [jnp.exp(gl_ref[i : i + 1, :]) for i in range(GROUPS)]
-    group_sum = sum(group_exp)
-    choice = [jnp.exp(cl_ref[j : j + 1, :]) for j in range(TOPK)]
-    expert_weight = [0.0] * group_size
-    for j in range(TOPK):
-        within = sum(over_groups(member[j] * member[i]) * choice[i] for i in range(TOPK))
-        prob = sum(member[j][i : i + 1, :] * group_exp[i] for i in range(GROUPS)) / group_sum
-        weight = prob * choice[j] / within
-        for m in range(group_size):
-            named = route[j] == group * group_size + m
-            expert_weight[m] = expert_weight[m] + jnp.where(named, weight, 0.0)
-    sub = lax.broadcasted_iota(jnp.int32, (8, rows), 0)
-    stacked = jnp.zeros((8, rows), F32)
-    for m in range(group_size):
-        for i, piece in enumerate(split3(expert_weight[m])):
-            stacked = jnp.where(sub == 3 * m + i, piece.astype(F32), stacked)
-    stacked = stacked.astype(BF16)
-
     tok_load.wait()
     egain_load.wait()
     tokens = tok_ref[...].astype(F32)
@@ -274,14 +254,7 @@
     for i in range(GROUPS):
         chosen = perm[i * cap : (i + 1) * cap, :]
         disp[i] = jnp.dot(chosen, normed, preferred_element_type=F32).astype(BF16)
-        got = nt_dot(stacked, chosen)
-        pair = [got[3 * m : 3 * m + 1, :] + got[3 * m + 1 : 3 * m + 2, :] + got[3 * m + 2 : 3 * m + 3, :]
-                for m in range(group_size)]
-        lanes = lax.broadcasted_iota(jnp.int32, (8, cap), 0)
-        packed = jnp.where(lanes == 0, pair[0], jnp.where(lanes == 1, pair[1], 0.0))
-        wsrc[i] = jnp.concatenate([packed, jnp.zeros((8, wsrc.shape[2] - cap), F32)], axis=1)
     flat[0, c, x] = disp[z]
-    wgot[0] = wsrc[z]
 
     pl.semaphore_wait(barrier, len(z_dev[1:]) + 3)
 
@@ -364,30 +337,38 @@
 
     depth = wd_ref.shape[0] // 4
 
-    def v_send(k):
-        return remote(vout.at[k, 1], vin.at[k], vs.at[k], vr.at[k], x_dev)
+    def pieces(k):
+        count = 2 if k == GROUPS - 1 else 1
+        size = vout.shape[3] // count
+        return [slice(j * size, (j + 1) * size) for j in range(count)]
+
+    def v_send(k, j):
+        at = pieces(k)[j]
+        return remote(vout.at[k, 1, :, at], vin.at[k, :, at], vs.at[k, j], vr.at[k, j], x_dev)
 
     def down(k):
         for i in range(2):
             hc_send(k, i, quarter_c, 0).wait_recv()
             hc_send(k, i, quarter_d, 1).wait_recv()
-        value = sum(
-            jnp.dot(
-                jnp.concatenate([hid[k, block[i], n] for i in range(2)], axis=0),
-                wd_ref[n * depth : (n + 1) * depth, :], preferred_element_type=F32,
-            )
-            for n in range(4)
-        ).astype(BF16)
-        vout[k, 0] = value[:cap]
-        vout[k, 1] = value[cap:]
-        v_send(k).start()
-
-    def r_send(k):
-        return remote(ret.at[k], back.at[z], rs.at[k], rr.at[k], z_dev[k])
-
-    def combine(k):
-        v_send(k).wait_recv()
-        if k > 0:
+        act = [jnp.concatenate([hid[k, block[i], n] for i in range(2)], axis=0) for n in range(4)]
+        for j, at in enumerate(pieces(k)):
+            value = sum(
+                jnp.dot(
+                    act[n], wd_ref[n * depth : (n + 1) * depth, at], preferred_element_type=F32
+                )
+                for n in range(4)
+            ).astype(BF16)
+            vout[k, 0, :, at] = value[:cap]
+            vout[k, 1, :, at] = value[cap:]
+            v_send(k, j).start()
+
+    def r_send(k, j):
+        at = pieces(k)[j]
+        return remote(ret.at[k, :, at], back.at[z, :, at], rs.at[k, j], rr.at[k, j], z_dev[k])
+
+    def combine(k, j=0):
+        v_send(k, j).wait_recv()
+        if k > 0 and j == 0:
             w_send(k).wait_recv()
         d0 = lax.broadcasted_iota(jnp.int32, (cap, cap), 0)
         d1 = lax.broadcasted_iota(jnp.int32, (cap, cap), 1)
@@ -398,14 +379,48 @@
         def column(row):
             return jnp.sum(jnp.where(d0 == d1, row, 0.0), axis=-1, keepdims=True)
 
+        at = pieces(k)[j]
         row = (
-            column(mine) * vout[k, 0].astype(F32) + column(theirs) * vin[k].astype(F32)
+            column(mine) * vout[k, 0, :, at].astype(F32)
+            + column(theirs) * vin[k, :, at].astype(F32)
         ).astype(BF16)
         if k == 0:
             back[z] = row
         else:
-            ret[k] = row
-            r_send(k).start()
+            ret[k, :, at] = row
+            r_send(k, j).start()
+
+    def weights():
+        gl_load.wait()
+        cl_load.wait()
+        group_exp = [jnp.exp(gl_ref[i : i + 1, :]) for i in range(GROUPS)]
+        group_sum = sum(group_exp)
+        choice = [jnp.exp(cl_ref[j : j + 1, :]) for j in range(TOPK)]
+        expert_weight = [0.0] * group_size
+        for j in range(TOPK):
+            within = sum(over_groups(member[j] * member[i]) * choice[i] for i in range(TOPK))
+            prob = sum(member[j][i : i + 1, :] * group_exp[i] for i in range(GROUPS)) / group_sum
+            weight = prob * choice[j] / within
+            for m in range(group_size):
+                named = route[j] == group * group_size + m
+                expert_weight[m] = expert_weight[m] + jnp.where(named, weight, 0.0)
+        sub = lax.broadcasted_iota(jnp.int32, (8, rows), 0)
+        stacked = jnp.zeros((8, rows), F32)
+        for m in range(group_size):
+            for i, piece in enumerate(split3(expert_weight[m])):
+                stacked = jnp.where(sub == 3 * m + i, piece.astype(F32), stacked)
+        stacked = stacked.astype(BF16)
+        for i in range(GROUPS):
+            chosen = perm[i * cap : (i + 1) * cap, :]
+            got = nt_dot(stacked, chosen)
+            pair = [got[3 * m : 3 * m + 1, :] + got[3 * m + 1 : 3 * m + 2, :] + got[3 * m + 2 : 3 * m + 3, :]
+                    for m in range(group_size)]
+            lanes = lax.broadcasted_iota(jnp.int32, (8, cap), 0)
+            packed = jnp.where(lanes == 0, pair[0], jnp.where(lanes == 1, pair[1], 0.0))
+            wsrc[i] = jnp.concatenate([packed, jnp.zeros((8, wsrc.shape[2] - cap), F32)], axis=1)
+        wgot[0] = wsrc[z]
+        for k in range(1, GROUPS):
+            w_send(k).start()
 
     length = q_ref.shape[0]
     heads = q_ref.shape[1] // KEYDIM
@@ -534,9 +549,8 @@
         z_send(k).start()
     x_send(0, x).start()
     c_send(0, 0, c).start()
-    for k in range(1, GROUPS):
-        w_send(k).start()
     payload()
+    weights()
     q_load.wait()
     rest(0)
     rest(1)
@@ -553,56 +567,59 @@
     arrive_z(1)
     gate_up((0, 1))
     arrive_d(0)
-    gate_up((1, 0))
     arrive_x(2)
+    gate_up((2, 0), (1, 0))
+    arrive_z(3)
     hop(1)
-    gate_up((2, 0))
+    arrive_x(1)
     arrive_y(0, 1)
-    arrive_x(1)
-    arrive_z(3)
-    arrive_y(1, 0)
+    gate_up((3, 0))
     arrive_d(1)
-    gate_up((1, 1), (3, 0))
     wd_load.wait()
     down(0)
+    gate_up((2, 1))
+    arrive_x(3)
     hop(2)
-    gate_up((2, 1))
     arrive_y(2, 0)
-    arrive_x(3)
-    arrive_y(1, 1)
+    arrive_y(1, 0)
+    gate_up((3, 1), (1, 1))
     hop(3)
     arrive_y(3, 0)
-    gate_up((3, 1))
+    arrive_y(2, 1)
     combine(0)
-    arrive_y(2, 1)
-    down(1)
     arrive_ent()
     g_load.wait()
     hgain_load.wait()
     finish(0)
+    down(2)
     finish(1)
-    down(2)
+    arrive_y(3, 1)
+    arrive_y(1, 1)
+    down(3)
+    down(1)
+    combine(2)
+    arrive_mix(0)
+    combine(3, 0)
+    combine(3, 1)
     combine(1)
-    arrive_y(3, 1)
-    combine(2)
-    down(3)
-    arrive_mix(0)
+    arrive_mix(1)
     proj_load.wait()
-    combine(3)
     project(0)
-    arrive_mix(1)
     project(1)
     for k in range(1, GROUPS):
-        r_send(k).wait_recv()
+        for j in range(len(pieces(k))):
+            r_send(k, j).wait_recv()
     expert_ref[...] = tn_dot(perm[...], back[...].reshape(slots, back.shape[2])).astype(BF16)
 
     for k in range(GROUPS):
         if k > 0:
             z_send(k).wait_send()
             w_send(k).wait_send()
-            r_send(k).wait_send()
+            for j in range(len(pieces(k))):
+                r_send(k, j).wait_send()
         x_send(k, x).wait_send()
-        v_send(k).wait_send()
+        for j in range(len(pieces(k))):
+            v_send(k, j).wait_send()
         for i in range(2):
             c_send(k, i, c).wait_send()
             y_send(k, i, own).wait_send()
@@ -682,7 +699,7 @@
             vmem((4, length, width), BF16),
             dma((15,)), dma((n,)), dma((n,)), dma((n,)), dma((n,)), dma((n,)), dma((n,)),
             dma((n, 2)), dma((n, 2)), dma((n, 2)), dma((n, 2)), dma((n, 2, 2)), dma((n, 2, 2)),
-            dma((n,)), dma((n,)), dma((n,)), dma((n,)),
+            dma((n, 2)), dma((n, 2)), dma((n, 2)), dma((n, 2)),
             dma, dma, dma, dma, dma, dma, dma((2,)), dma((2,)), dma((2, 2)), dma((2, 2)),
             dma((2,)), dma((2,)),
         ],

time: 43 us -> 40.4 us (0.940)
  Pallas kernels: 42.2 us -> 39.6 us
    pallas_call x1, Pallas kernels: 41.5 us -> 38.9 us  [fused(): pl.pallas_call(fused_kernel, name='fused', out_shape=(vmem((length, mixer...]
where the time goes in v3:
time: 40.4 us; the launch traced here: 40.3 us
  Pallas kernels  39.6 us (98%)
  between operations  0.64 us (2%)
    pallas_call x1, Pallas kernels, fused(): pl.pallas_call(fused_kernel, name='fused', out_shape=(vmem((length, mixer...  38.9 us

profile of v3, /device:TPU:0, one launch (start us, length us, event | category | flops | bytes accessed | tf_op | source)
XLA Modules:
  0.0 40.3 jit_solution(13269241290305622820)
XLA Ops:
  0.6 38.9 %fused.1 = (bf16[256,512]{1,0:T(8,128)(2,1)S(1)}, bf16[128,512]{1,0:T(8,128)(2,1)S(1)}) custom-call(s32[2,128]{1,0:T(2,128)} %bitcast.15, f32[4,128]{1,0:T(4,128)} %bitcast.13, f32[2,128]{1,0:T(2,128)} %bitcast.16, f32[1,512]{1,0:T(1,128)} %bitcast.14, f32[1,128]{1,0:T(1,128)} %bitcast.17, f32[1,2048]{1,0:T(1,128)} %bitcast.12, bf16[256,512]{1,0:T(8,128)(2,1)} %q_hbm.1, ...), custom_call_target="tpu_custom_call" | custom-call | flops 8000000000 | bytes 12000000 | tf_op jit(solution)/shard_map/fused/pallas_call | solution.py:668
  39.5 0.8 %emit.1 = (bf16[256,512]{1,0:T(8,128)(2,1)}, bf16[128,512]{1,0:T(8,128)(2,1)}) custom-call(bf16[256,512]{1,0:T(8,128)(2,1)S(1)} %get-tuple-element.4.mixer_ref, bf16[128,512]{1,0:T(8,128)(2,1)S(1)} %get-tuple-element.5.expert_ref), custom_call_target="tpu_custom_call" | custom-call | flops 1000000 | bytes 800000 | tf_op jit(solution)/shard_map/emit/pallas_call | solution.py:715

commit v4 on v3

--- a/solution.py
+++ b/solution.py
@@ -531,6 +531,13 @@
         m_send(j, own).start()
         mc_send(j, own, 0).start()
 
+    def finish_when(ready):
+        @pl.when(ready)
+        def _():
+            arrive_ent()
+            finish(0)
+            finish(1)
+
     def arrive_mix(j):
         m_send(j, quarter_y).wait_recv()
         mc_send(j, quarter_y, 1).start()
@@ -565,43 +572,42 @@
     hop(0)
     arrive_y(0, 0)
     arrive_z(1)
-    gate_up((0, 1))
+    gate_up((1, 0))
     arrive_d(0)
     arrive_x(2)
-    gate_up((2, 0), (1, 0))
     arrive_z(3)
+    gate_up((2, 0))
     hop(1)
     arrive_x(1)
-    arrive_y(0, 1)
+    arrive_y(1, 0)
     gate_up((3, 0))
     arrive_d(1)
+    gate_up((2, 1), (1, 1))
     wd_load.wait()
-    down(0)
-    gate_up((2, 1))
+    hop(2)
     arrive_x(3)
-    hop(2)
     arrive_y(2, 0)
-    arrive_y(1, 0)
-    gate_up((3, 1), (1, 1))
+    gate_up((3, 1), (0, 1))
     hop(3)
     arrive_y(3, 0)
-    arrive_y(2, 1)
-    combine(0)
-    arrive_ent()
     g_load.wait()
     hgain_load.wait()
-    finish(0)
+    arrive_y(2, 1)
+    finish_when(z < GROUPS - 1)
+    arrive_y(1, 1)
     down(2)
-    finish(1)
     arrive_y(3, 1)
-    arrive_y(1, 1)
+    finish_when(z == GROUPS - 1)
     down(3)
+    combine(2)
+    arrive_y(0, 1)
     down(1)
-    combine(2)
-    arrive_mix(0)
+    down(0)
     combine(3, 0)
     combine(3, 1)
     combine(1)
+    arrive_mix(0)
+    combine(0)
     arrive_mix(1)
     proj_load.wait()
     project(0)

time: 40.4 us -> 40 us (0.990)
    pallas_call x1, Pallas kernels: 38.9 us -> 38.4 us  [fused(): pl.pallas_call(fused_kernel, name='fused', out_shape=(vmem((length, mixer...]
where the time goes in v4:
time: 40 us; the launch traced here: 39.8 us
  Pallas kernels  39.2 us (98%)
  between operations  0.64 us (2%)
    pallas_call x1, Pallas kernels, fused(): pl.pallas_call(fused_kernel, name='fused', out_shape=(vmem((length, mixer...  38.4 us

profile of v4, /device:TPU:0, one launch (start us, length us, event | category | flops | bytes accessed | tf_op | source)
XLA Modules:
  0.0 39.8 jit_solution(1432198454946458782)
XLA Ops:
  0.6 38.4 %fused.1 = (bf16[256,512]{1,0:T(8,128)(2,1)S(1)}, bf16[128,512]{1,0:T(8,128)(2,1)S(1)}) custom-call(s32[2,128]{1,0:T(2,128)} %bitcast.15, f32[4,128]{1,0:T(4,128)} %bitcast.13, f32[2,128]{1,0:T(2,128)} %bitcast.16, f32[1,512]{1,0:T(1,128)} %bitcast.14, f32[1,128]{1,0:T(1,128)} %bitcast.17, f32[1,2048]{1,0:T(1,128)} %bitcast.12, bf16[256,512]{1,0:T(8,128)(2,1)} %q_hbm.1, ...), custom_call_target="tpu_custom_call" | custom-call | flops 8000000000 | bytes 12000000 | tf_op jit(solution)/shard_map/fused/pallas_call | solution.py:674
  39.1 0.8 %emit.1 = (bf16[256,512]{1,0:T(8,128)(2,1)}, bf16[128,512]{1,0:T(8,128)(2,1)}) custom-call(bf16[256,512]{1,0:T(8,128)(2,1)S(1)} %get-tuple-element.4.mixer_ref, bf16[128,512]{1,0:T(8,128)(2,1)S(1)} %get-tuple-element.5.expert_ref), custom_call_target="tpu_custom_call" | custom-call | flops 1000000 | bytes 800000 | tf_op jit(solution)/shard_map/emit/pallas_call | solution.py:721
